TPU v7x, 32 devices: a whole 2x2x4 slice. The times are simulated.
32 devices in a mesh: sp: 8 (over z, y), tp: 4 (over x, core).
Axes of the slice: x: 2, y: 2, z: 4, core: 2. Of those that a mesh axis runs over, the one named last changes fastest.
Arguments:
- stream: bfloat16 [3072, 2048], P(('sp', 'tp')), may hold values from -6 to 6
- query_nope: bfloat16 [3072, 16, 128], P('sp', 'tp'), may hold values from -6 to 6
- query_rope: bfloat16 [3072, 16, 64], P('sp', 'tp'), may hold values from -700 to 700
- latent: bfloat16 [3072, 512], P('sp'), may hold values from -6 to 6
- rope_key: bfloat16 [3072, 64], P('sp'), may hold values from -6 to 6
- latent_gain: float32 [512], replicated, may hold values from 0.1 to 1.9
- key_up: bfloat16 [512, 16, 128], P(None, 'tp'), may hold values from -0.375 to 0.375
- value_up: bfloat16 [512, 16, 128], P(None, 'tp'), may hold values from -2.6516504 to 2.6516504
- out_gain: float32 [2048], P('tp'), may hold values from 0.1 to 1.9
- out_weight: bfloat16 [2048, 2048], P('tp'), may hold values from -0.125 to 0.125
- norm_gain: float32 [2048], replicated, may hold values from 0.1 to 1.9
- ff_in: bfloat16 [2048, 8192], P('sp', 'tp'), may hold values from -0.125 to 0.125
- ff_out: bfloat16 [8192, 2048], P('tp', 'sp'), may hold values from -0.0625 to 0.0625
Outputs:
- layer_out: bfloat16 [3072, 2048], P(('sp', 'tp'))
All inputs are finite; a program needn't handle non-finite values.
Results may differ from a plain program's by a relative error of at most 0.018.
Values may be sent and summed in bfloat16 or wider, within the bound.
A program may use at most 128 MiB of HBM per device.

v0:
```python
import math

import jax
import jax.numpy as jnp
from jax import lax
from jax.sharding import PartitionSpec as P

HEADS = 16
NOPE = 128
ROPE = 64
LATENT = 512
VDIM = 128


EPS = 1e-06
THETA = 10000.0


def turn(values, positions):
    full_width = values.shape[-1]
    half_width = full_width // 2
    inverse = jnp.power(THETA, -jnp.arange(0, full_width, 2, dtype=jnp.float32) / full_width)
    angles = positions[:, None] * inverse[None, :]
    cosine = jnp.cos(angles)
    sine_part = jnp.sin(angles)
    if values.ndim == 3:
        cosine = cosine[:, None, :]
        sine_part = sine_part[:, None, :]
    vector = values.astype(jnp.float32)
    lower_half = vector[..., :half_width]
    upper_half = vector[..., half_width:]
    return jnp.concatenate(
        [
            lower_half * cosine - upper_half * sine_part,
            lower_half * sine_part + upper_half * cosine,
        ],
        axis=-1,
    )


def body(
    stream,
    query_nope,
    query_rope,
    latent,
    rope_key,
    latent_gain,
    key_up,
    value_up,
    out_gain,
    out_weight,
    norm_gain,
    ff_in,
    ff_out,
):
    local_rows = query_nope.shape[0]
    local_heads = query_nope.shape[1]
    row_start = lax.axis_index("sp") * local_rows
    positions = (row_start + jnp.arange(local_rows, dtype=jnp.int32)).astype(jnp.float32)
    lat_full = latent.astype(jnp.float32)
    normed = (
        lat_full
        * lax.rsqrt(jnp.mean(lat_full * lat_full, axis=-1, keepdims=True) + EPS)
        * latent_gain
    ).astype(jnp.bfloat16)
    keys_rot = turn(rope_key, positions).astype(jnp.bfloat16)
    query_rot = turn(query_rope, positions).astype(jnp.bfloat16)
    query_lat = jnp.einsum(
        "thn,lhn->thl", query_nope, key_up, preferred_element_type=jnp.float32
    ).astype(jnp.bfloat16)
    score_scale = 1.0 / math.sqrt(NOPE + ROPE)

    def fold_block(running, lat_block, rot_block):
        running_max, running_sum, accum = running
        scores = (
            jnp.einsum("thl,kl->thk", query_lat, lat_block, preferred_element_type=jnp.float32)
            + jnp.einsum("thr,kr->thk", query_rot, rot_block, preferred_element_type=jnp.float32)
        ) * score_scale
        new_max = jnp.maximum(running_max, jnp.max(scores, axis=-1))
        fading = jnp.exp(running_max - new_max)
        expo = jnp.exp(scores - new_max[..., None])
        running_sum = running_sum * fading + jnp.sum(expo, axis=-1)
        accum = accum * fading[..., None] + jnp.einsum(
            "thk,kl->thl", expo.astype(jnp.bfloat16), lat_block, preferred_element_type=jnp.float32
        )
        return (new_max, running_sum, accum)

    initial = (
        jnp.full((local_rows, local_heads), -1e30, jnp.float32),
        jnp.zeros((local_rows, local_heads), jnp.float32),
        jnp.zeros((local_rows, local_heads, LATENT), jnp.float32),
    )
    lat_piece = lax.all_gather(normed, "sp", axis=0, tiled=True)
    key_piece = lax.all_gather(keys_rot, "sp", axis=0, tiled=True)
    key_count = lat_piece.shape[0]
    key_block = math.gcd(key_count, 2048)
    lat_blocks = lat_piece.reshape(key_count // key_block, key_block, lat_piece.shape[1])
    key_blocks = key_piece.reshape(key_count // key_block, key_block, key_piece.shape[1])

    def advance(running, block_pair):
        return (fold_block(running, block_pair[0], block_pair[1]), None)

    result, _ = lax.scan(advance, initial, (lat_blocks, key_blocks))
    running_max, running_sum, accum = result
    out_lat = (accum / running_sum[..., None]).astype(jnp.bfloat16)
    head_out = jnp.einsum("thl,lhv->thv", out_lat, value_up, preferred_element_type=jnp.float32)
    square_sums = lax.psum(jnp.sum(head_out * head_out, axis=(1, 2)), "tp")
    row_scale = lax.rsqrt(square_sums / (HEADS * VDIM) + EPS)
    gated = (head_out.reshape(local_rows, local_heads * VDIM) * out_gain).astype(jnp.bfloat16)
    row_share = local_rows // lax.axis_size("tp")
    projected = lax.psum_scatter(
        jnp.dot(gated, out_weight, preferred_element_type=jnp.float32).astype(jnp.bfloat16),
        "tp",
        scatter_dimension=0,
        tiled=True,
    ).astype(jnp.float32)
    own_scale = lax.dynamic_slice_in_dim(row_scale, lax.axis_index("tp") * row_share, row_share, 0)
    mid_stream = stream.astype(jnp.float32) + own_scale[:, None] * projected
    ff_input = (
        mid_stream
        * lax.rsqrt(jnp.mean(mid_stream * mid_stream, axis=-1, keepdims=True) + EPS)
        * norm_gain
    ).astype(jnp.bfloat16)
    all_rows = lax.all_gather(ff_input, "tp", axis=0, tiled=True)
    pre_act = jnp.dot(
        all_rows,
        lax.all_gather(ff_in, "sp", axis=0, tiled=True),
        preferred_element_type=jnp.float32,
    )
    activation = jnp.square(jax.nn.relu(pre_act)).astype(jnp.bfloat16)
    ff_whole = lax.all_gather(ff_out, "sp", axis=1, tiled=True)
    mixed = lax.psum_scatter(
        jnp.dot(activation, ff_whole, preferred_element_type=jnp.float32).astype(jnp.bfloat16),
        "tp",
        scatter_dimension=0,
        tiled=True,
    ).astype(jnp.float32)
    return (mid_stream + mixed).astype(jnp.bfloat16)


def solution(mesh):
    placed = (
        P(("sp", "tp"), None),
        P("sp", "tp", None),
        P("sp", "tp", None),
        P("sp", None),
        P("sp", None),
        P(),
        P(None, "tp", None),
        P(None, "tp", None),
        P("tp"),
        P("tp", None),
        P(),
        P("sp", "tp"),
        P("tp", "sp"),
    )
    return jax.shard_map(
        body, mesh=mesh, in_specs=placed, out_specs=P(("sp", "tp"), None), check_vma=False
    )
```

profile of v0, /device:TPU:0, one launch (start us, length us, event | category | flops | bytes accessed | tf_op | source)
XLA Modules:
  0.0 483.3 jit_solution(7457804570286899797)
XLA Ops:
  6.5 0.0 copy-start
  6.5 0.0 copy-start.4
  6.5 0.0 all-gather.5.cloned.1.call-start
  6.5 1.3 fusion.22
  7.9 1.9 fusion.24
  9.8 0.0 all-gather.5.cloned.1.call-update
  9.8 0.0 reduce-scatter.3.cloned.1.call-start
  9.9 0.8 convert_element_type.65
  10.7 1.0 convert_element_type.67
  11.7 0.3 multiply_cosine_fusion
  12.0 34.4 %all_gather.16 = bf16[3072,64]{0,1:T(8,128)(2,1)S(1)} all-gather(bf16[384,64]{0,1:T(8,128)(2,1)S(1)} %pad_maximum_fusion.1), channel_id=1, replica_groups=mesh['sp'=8,'tp'=4] {'sp'}, dimensions={0}, use_global_device_ids=true | all-gather | bytes 442368 | tf_op jit(solution)/shard_map/all_gather | solution.py:94
  46.4 0.0 copy-done.4
  46.4 2.7 fusion.21
  49.2 2.6 copy.22
  51.8 0.1 subtract_convert_fusion
  51.8 23.7 %all-gather.5.cloned.1.call-done = bf16[3072,512]{1,0:T(8,128)(2,1)} async-done(((bf16[384,512]{1,0:T(8,128)(2,1)}), bf16[3072,512]{1,0:T(8,128)(2,1)}) %all-gather.5.cloned.1.call-update) | async-done | bytes 3145744 | tf_op jit(solution)/shard_map/all_gather | solution.py:93
  75.5 51.9 %while.15 = (s32[]{:T(128)}, f32[384,4]{0,1:T(4,128)S(1)}, f32[384,4]{0,1:T(4,128)S(1)}, f32[384,4,512]{2,0,1:T(8,128)}, bf16[3,1024,512]{2,1,0:T(8,128)(2,1)}, ...) while((s32[]{:T(128)}, f32[384,4]{0,1:T(4,128)S(1)}, ...), condition=%wide.region_4.5_spmd.clone, body=%wide.region_1.4_spmd.clone.sunk | while | flops 3435929088 | bytes 67011724 | solution.py:103
  75.5 3.6 fusion.52
  79.1 3.7 bitcast_reduce_fusion.2
  82.8 3.8 fusion.53
  86.6 0.8 copy-done.1
  87.4 4.8 fusion.55
  92.2 3.6 fusion.52
  95.7 3.7 bitcast_reduce_fusion.2
  99.5 3.8 fusion.53
  103.2 0.8 copy-done.1
  104.0 5.8 %fusion.55 = f32[384,4,512]{2,0,1:T(8,128)} fusion(f32[384,4,512]{2,0,1:T(8,128)} %get-tuple-element.193, f32[384,4]{0,1:T(4,128)S(1)} %get-tuple-element.179, pred[]{:T(512)S(6)} %compare.3, f32[1024,384,4]{1,0,2:T(8,128)S(1)} %copy-done.1, f32[384,4]{0,1:T(4,128)S(1)} %select_maximum_fusion.2, bf16[3,1024,512]{2,1,0:T(8,128)(2,1)} %get-tuple-element.204, ...), kind=kOutput, calls=%fused_computation.8.clone.1 | convolution fusion | flops 1616117760 | bytes 13644289 | tf_op jit(solution)/shard_map/while/body/eval_jaxpr/thk,kl->thl/dot_general | solution.py:83
  109.8 3.6 fusion.52
  113.4 3.7 bitcast_reduce_fusion.2
  117.1 3.8 fusion.53
  120.9 0.8 copy-done.1
  121.7 5.7 %fusion.55 = f32[384,4,512]{2,0,1:T(8,128)} fusion(f32[384,4,512]{2,0,1:T(8,128)} %get-tuple-element.193, f32[384,4]{0,1:T(4,128)S(1)} %get-tuple-element.179, pred[]{:T(512)S(6)} %compare.3, f32[1024,384,4]{1,0,2:T(8,128)S(1)} %copy-done.1, f32[384,4]{0,1:T(4,128)S(1)} %select_maximum_fusion.2, bf16[3,1024,512]{2,1,0:T(8,128)(2,1)} %get-tuple-element.204, ...), kind=kOutput, calls=%fused_computation.8.clone.1 | convolution fusion | flops 1616117760 | bytes 13644289 | tf_op jit(solution)/shard_map/while/body/eval_jaxpr/thk,kl->thl/dot_general | solution.py:83
  127.4 0.0 copy-done.7
  127.4 2.7 fusion.26
  130.1 0.0 copy-done.6
  130.1 0.0 copy-start.2
  130.1 0.1 fusion.25
  130.3 0.0 copy-done
  130.3 0.0 copy-start.5
  130.3 2.2 convolution_convert_fusion.1
  132.5 0.0 reduce-scatter.3.cloned.1.call-update
  132.5 0.0 all-gather.7.cloned.1.call-start
  132.5 5.7 %psum.7 = f32[384]{0:T(512)S(1)} all-reduce(f32[384]{0:T(512)S(1)} %get-tuple-element.121), channel_id=1, replica_groups=mesh['sp'=8,'tp'=4] {'tp'}, use_global_device_ids=true, to_apply=%region_6.7 | all-reduce | flops 384 | bytes 3072 | tf_op jit(solution)/shard_map/psum | solution.py:107
  138.2 0.1 dynamic_slice.11
  138.3 21.0 %reduce-scatter.3.cloned.1.call-done = bf16[96,2048]{1,0:T(8,128)(2,1)} async-done(((bf16[384,2048]{1,0:T(8,128)(2,1)}), bf16[96,2048]{1,0:T(8,128)(2,1)}) %reduce-scatter.3.cloned.1.call-update) | async-done | bytes 393232 | tf_op jit(solution)/shard_map/reduce_scatter | solution.py:111
  159.3 0.0 copy-done.2
  159.3 1.3 multiply_reduce_fusion
  160.6 0.0 copy-done.5
  160.6 2.0 multiply_convert_fusion.1
  162.7 0.0 all-gather.7.cloned.1.call-update
  162.7 0.0 all-gather.11.cloned.1.call-start
  162.7 0.5 all-gather.11.cloned.1.call-update
  163.3 0.0 all-gather.9.cloned.1.call-start
  163.3 0.5 all-gather.9.cloned.1.call-update
  163.9 0.0 copy-start.3
  163.9 0.2 reduce-scatter.5.cloned.1.call-start
  164.1 18.4 %all-gather.7.cloned.1.call-done = bf16[384,2048]{1,0:T(8,128)(2,1)} async-done(((bf16[96,2048]{1,0:T(8,128)(2,1)}), bf16[384,2048]{1,0:T(8,128)(2,1)}) %all-gather.7.cloned.1.call-update) | async-done | bytes 1572880 | tf_op jit(solution)/shard_map/all_gather | solution.py:124
  182.5 126.9 %all-gather.11.cloned.1.call-done = bf16[2048,2048]{1,0:T(8,128)(2,1)} async-done(((bf16[2048,256]{1,0:T(8,128)(2,1)}), bf16[2048,2048]{1,0:T(8,128)(2,1)}) %all-gather.11.cloned.1.call-update) | async-done | bytes 8388624 | tf_op jit(solution)/shard_map/all_gather | solution.py:131
  309.4 124.7 %all-gather.9.cloned.1.call-done = bf16[2048,2048]{1,0:T(8,128)(2,1)} async-done(((bf16[256,2048]{1,0:T(8,128)(2,1)}), bf16[2048,2048]{1,0:T(8,128)(2,1)}) %all-gather.9.cloned.1.call-update) | async-done | bytes 8388624 | tf_op jit(solution)/shard_map/all_gather | solution.py:127
  434.0 14.0 %convolution_convert_fusion = bf16[384,2048]{1,0:T(8,128)(2,1)} fusion(bf16[2048,2048]{1,0:T(8,128)(2,1)} %all-gather.11.cloned.1.call-done, bf16[384,2048]{1,0:T(8,128)(2,1)} %all-gather.7.cloned.1.call-done, bf16[2048,2048]{1,0:T(8,128)(2,1)} %all-gather.9.cloned.1.call-done), kind=kOutput, calls=%fused_computation.26 | convolution fusion | flops 6445596672 | bytes 19922944 | tf_op jit(solution)/shard_map/dot_general | solution.py:133
  448.0 0.0 reduce-scatter.5.cloned.1.call-update
  448.1 26.4 %reduce-scatter.5.cloned.1.call-done = bf16[96,2048]{1,0:T(8,128)(2,1)} async-done(((bf16[384,2048]{1,0:T(8,128)(2,1)}), bf16[96,2048]{1,0:T(8,128)(2,1)}) %reduce-scatter.5.cloned.1.call-update) | async-done | bytes 393232 | tf_op jit(solution)/shard_map/reduce_scatter | solution.py:132
  474.5 0.0 copy-done.3
  474.5 2.0 add_convert_fusion
  (25 shorter events, 0.2 us)
Async XLA Ops:
  6.5 123.7 %copy-start = (bf16[512,2048]{1,0:T(8,128)(2,1)S(1)}, bf16[512,2048]{1,0:T(8,128)(2,1)}, u32[]{:S(2)}) copy-start(bf16[512,2048]{1,0:T(8,128)(2,1)} %param.24) | copy-start | bytes 6291460
  6.5 39.9 %copy-start.4 = (bf16[512,4,128]{2,1,0:T(4,128)(2,1)S(1)}, bf16[512,4,128]{2,1,0:T(4,128)(2,1)}, u32[]{:S(2)}) copy-start(bf16[512,4,128]{2,1,0:T(4,128)(2,1)} %param.21) | copy-start | bytes 1572868
  6.5 69.0 %all-gather.5.cloned.1.call-start = ((), (), s32[]{:S(2)}) async-start(), calls=%async_computation.2 | async-start | bytes 3538944 | tf_op jit(solution)/shard_map/all_gather | solution.py:93
  9.8 149.5 %reduce-scatter.3.cloned.1.call-start = ((), (), s32[]{:S(2)}) async-start(), calls=%async_computation.3 | async-start | bytes 1966080 | tf_op jit(solution)/shard_map/reduce_scatter | solution.py:111
  75.5 51.9 %copy-start.7 = (bf16[512,4,128]{2,1,0:T(4,128)(2,1)S(1)}, bf16[512,4,128]{2,1,0:T(4,128)(2,1)}, u32[]{:S(2)}) copy-start(bf16[512,4,128]{2,1,0:T(4,128)(2,1)} %param.22) | copy-start | bytes 1572868
  82.8 4.6 copy-start.1
  99.4 4.6 copy-start.1
  117.1 4.6 copy-start.1
  127.4 2.7 copy-start.6
  130.1 29.2 %copy-start.2 = (bf16[96,2048]{1,0:T(8,128)(2,1)S(1)}, bf16[96,2048]{1,0:T(8,128)(2,1)}, u32[]{:S(2)}) copy-start(bf16[96,2048]{1,0:T(8,128)(2,1)} %param.15) | copy-start | bytes 1179652
  130.3 30.3 %copy-start.5 = (f32[2048]{0:T(1024)S(1)}, f32[2048]{0:T(1024)}, u32[]{:S(2)}) copy-start(f32[2048]{0:T(1024)} %param.25) | copy-start | bytes 24580
  132.5 50.0 %all-gather.7.cloned.1.call-start = ((), (), s32[]{:S(2)}) async-start(), calls=%async_computation.4 | async-start | bytes 1966080 | tf_op jit(solution)/shard_map/all_gather | solution.py:124
  162.7 146.7 %all-gather.11.cloned.1.call-start = ((), (), s32[]{:S(2)}) async-start(), calls=%async_computation.6 | async-start | bytes 9437184 | tf_op jit(solution)/shard_map/all_gather | solution.py:131
  163.3 270.7 %all-gather.9.cloned.1.call-start = ((), (), s32[]{:S(2)}) async-start(), calls=%async_computation.5 | async-start | bytes 9437184 | tf_op jit(solution)/shard_map/all_gather | solution.py:127
  163.9 310.6 %copy-start.3 = (bf16[96,2048]{1,0:T(8,128)(2,1)S(1)}, bf16[96,2048]{1,0:T(8,128)(2,1)}, u32[]{:S(2)}) copy-start(bf16[96,2048]{1,0:T(8,128)(2,1)} %reduce-scatter.3.cloned.1.call-done) | copy-start | bytes 1179652
  163.9 310.6 %reduce-scatter.5.cloned.1.call-start = ((), (), s32[]{:S(2)}) async-start(), calls=%async_computation.7 | async-start | bytes 1966080 | tf_op jit(solution)/shard_map/reduce_scatter | solution.py:132
Sparse Core Ops, SparseCore 0:
  9.9 65.5 all-gather.4
  132.6 26.6 reduce-scatter.2
  162.8 19.6 all-gather.6
  184.4 124.9 all-gather.10
  311.3 122.6 all-gather.8
  448.2 26.2 reduce-scatter.4
where the time goes:
time: 484 us; the launch traced here: 483 us
  waiting for transfers between devices  342 us (71%)
  matrix products  59.7 us (12%)
  blocking collectives  40.1 us (8%)
  other arithmetic  22.2 us (5%)
  between operations  13.6 us (3%)
  local copies, waits for them, and re-layouts  5.15 us (1%)
    all_gather x1, waiting for transfers between devices, body(): ff_whole = lax.all_gather(ff_out, 'sp', axis=1, tiled=True)  127 us
    all_gather x1, waiting for transfers between devices, body(): lax.all_gather(ff_in, 'sp', axis=0, tiled=True)  125 us
    all_gather x1, blocking collectives, body(): key_piece = lax.all_gather(keys_rot, 'sp', axis=0, tiled=True)  34.4 us
    reduce_scatter x1, waiting for transfers between devices, body(): lax.psum_scatter(jnp.dot(activation, ff_whole, preferred_element_type=jnp...  26.4 us
    all_gather x1, waiting for transfers between devices, body(): lat_piece = lax.all_gather(normed, 'sp', axis=0, tiled=True)  23.7 us
    reduce_scatter x1, waiting for transfers between devices, body(): lax.psum_scatter(jnp.dot(gated, out_weight, preferred_element_type=jnp.fl...  21 us
    all_gather x1, waiting for transfers between devices, body(): all_rows = lax.all_gather(ff_input, 'tp', axis=0, tiled=True)  18.4 us
    dot_general x3, matrix products, fold_block(): jnp.einsum('thk,kl->thl', expo.astype(jnp.bfloat16), lat_block, preferred...  16.3 us
  transfers between devices with their start and end apart: 6, of which 6 were waited for; matrix products, arithmetic and copies ran while one was open for 2% of the time, Pallas kernels for 0%

commit v1 on v0

v1 whole, which is shorter than its diff:
```python
import functools
import math

import jax
import jax.numpy as jnp
from jax import lax
from jax.experimental import pallas as pl
from jax.experimental.pallas import tpu as pltpu
from jax.sharding import PartitionSpec as P

EPS = 1e-06
THETA = 10000.0
F32 = jnp.float32
BF16 = jnp.bfloat16
MESH = pl.DeviceIdType.MESH
LANES = 128


def turn(values, positions):
    full_width = values.shape[-1]
    half_width = full_width // 2
    inverse = jnp.power(THETA, -jnp.arange(0, full_width, 2, dtype=F32) / full_width)
    angles = positions[:, None] * inverse[None, :]
    cosine = jnp.cos(angles)
    sine_part = jnp.sin(angles)
    if values.ndim == 3:
        cosine = cosine[:, None, :]
        sine_part = sine_part[:, None, :]
    vector = values.astype(F32)
    lower_half = vector[..., :half_width]
    upper_half = vector[..., half_width:]
    return jnp.concatenate(
        [
            lower_half * cosine - upper_half * sine_part,
            lower_half * sine_part + upper_half * cosine,
        ],
        axis=-1,
    )


def ring_shape(n):
    rows = 1
    while rows * rows < n:
        rows *= 2
    return (rows, n // rows) if n % rows == 0 else (n, 1)


def ring_pos(n, index):
    nz, ny = ring_shape(n)
    if ny == 1:
        return index
    z, y = index // ny, index % ny
    r = nz - 1 - z
    odd = r % 2
    c = (1 - odd) * (y - 1) + odd * (ny - 1 - y)
    return jnp.where(y == 0, z, nz + r * (ny - 1) + c)


def ring_at(n, pos):
    nz, ny = ring_shape(n)
    if ny == 1:
        return pos
    q = jnp.maximum(pos - nz, 0)
    r, c = q // (ny - 1), q % (ny - 1)
    odd = r % 2
    y = 1 + (1 - odd) * c + odd * (ny - 2 - c)
    return jnp.where(pos < nz, pos * ny, (nz - 1 - r) * ny + y)


def kernel(
    n, tp, heads, latent_width, width,
    kv_ref, q_ref, vup_ref, gain_ref, ow_ref, stream_ref, ngain_ref, ffin_ref, ffout_ref,
    out_ref,
    kv, fi, fo, ow, sc, acc, gated, proj, red, sq_out, sq_in, mid, xs, act, mixed, mix_out, mix_in,
    local_sem, lat_send, lat_recv, par_send, par_recv, w_send, w_recv,
    t_send, t_recv, m_send, m_recv,
):
    sp = lax.axis_index("sp")
    me = lax.axis_index("tp")
    pos = ring_pos(n, sp)
    rows = stream_ref.shape[0] * tp
    share = rows // tp
    total = width
    hidden = act.shape[1]
    dblk = total // n
    keys = kv.shape[0]
    core = me % 2
    partner = me + 1 - 2 * core

    def at(offset):
        return ring_at(n, lax.rem(pos + offset + n, n))

    right, left = at(1), at(-1)
    towards = (right, left)

    def peer(j):
        return lax.rem(me + j, tp)

    local = [
        pltpu.make_async_copy(ffin_ref, fi.at[pl.ds(sp * dblk, dblk)], local_sem.at[0]),
        pltpu.make_async_copy(ffout_ref, fo.at[sp], local_sem.at[1]),
        pltpu.make_async_copy(ow_ref, ow, local_sem.at[2]),
        pltpu.make_async_copy(kv_ref, kv.at[pl.ds(sp * rows, rows)], local_sem.at[3]),
    ]
    for c in (3, 0, 1, 2):
        local[c].start()

    barrier = pltpu.get_barrier_semaphore()
    for d in towards:
        pl.semaphore_signal(barrier, inc=1, device_id=(d, me), device_id_type=MESH)
    for j in range(1, tp):
        pl.semaphore_signal(barrier, inc=1, device_id=(sp, peer(j)), device_id_type=MESH)
    pl.semaphore_wait(barrier, tp + 1)

    quarter = rows // 4

    def lat_piece(src, way, c):
        return kv.at[pl.ds(src * rows + (2 * c + way) * quarter, quarter)]

    def came(way, step):
        return at(-1 - step) if way == 0 else at(1 + step)

    def going(way, step):
        return at(-step) if way == 0 else at(step)

    def lat_copy(way, step):
        ref = lat_piece(going(way, step), way, core)
        return pltpu.make_async_remote_copy(
            ref, ref, lat_send.at[way, step], lat_recv.at[way, step],
            device_id=(towards[way], me), device_id_type=MESH)

    def lat_wait(way, step):
        ref = lat_piece(came(way, step), way, core)
        pltpu.make_async_remote_copy(
            ref, ref, lat_send.at[way, step], lat_recv.at[way, step],
            device_id=(towards[way], me), device_id_type=MESH).wait_recv()

    def par_copy(way, step, c):
        ref = lat_piece(came(way, step), way, c)
        return pltpu.make_async_remote_copy(
            ref, ref, par_send.at[way, step], par_recv.at[way, step],
            device_id=(sp, partner), device_id_type=MESH)

    def w_piece(buf, src, way, sub):
        if buf == 0:
            part = dblk // 4
            return fi.at[pl.ds(src * dblk + (2 * way + sub) * part, part)]
        part = hidden // 4
        return fo.at[src, pl.ds((2 * way + sub) * part, part)]

    def w_copy(buf, way, sub, step):
        ref = w_piece(buf, going(way, step), way, sub)
        return pltpu.make_async_remote_copy(
            ref, ref, w_send.at[buf, way, sub, step], w_recv.at[buf, way, sub, step],
            device_id=(towards[way], me), device_id_type=MESH)

    def w_wait(buf, way, sub, step):
        ref = w_piece(buf, came(way, step), way, sub)
        pltpu.make_async_remote_copy(
            ref, ref, w_send.at[buf, way, sub, step], w_recv.at[buf, way, sub, step],
            device_id=(towards[way], me), device_id_type=MESH).wait_recv()

    def advance(buf, step):
        for sub in range(2):
            for way in range(2):
                if step > 0:
                    w_wait(buf, way, sub, step - 1)
                if step < n - 1:
                    w_copy(buf, way, sub, step).start()

    local[3].wait()
    for way in range(2):
        lat_copy(way, 0).start()
    local[0].wait()
    local[1].wait()
    for step in range(n - 1):
        for way in range(2):
            lat_wait(way, step)
            if step < n - 2:
                lat_copy(way, step + 1).start()
            par_copy(way, step, core).start()
        if step == n - 3:
            advance(0, 0)
    for step in range(n - 1):
        for way in range(2):
            par_copy(way, step, 1 - core).wait_recv()

    hops = [(0, s) for s in range(1, n)] + [(1, s) for s in range(0, n)]
    cursor = [0]

    def hop():
        buf, step = hops[cursor[0]]
        if buf == 0 and step == n - 1:
            cursor[0] += 1
            advance(1, 0)
            advance(0, n - 1)
            cursor[0] += 1
            return
        advance(buf, step)
        cursor[0] += 1

    scale = 1.0 / math.sqrt(LANES + (q_ref.shape[2] - latent_width) // 2)
    chunk = sc.shape[2]
    chunks = keys // chunk
    vdim = LANES
    squares = jnp.zeros((rows, 1), F32)
    fi_hops = n - 1
    points = 2 * heads
    for h in range(heads):
        def score(c, top):
            s = lax.dot_general(
                q_ref[h], kv[pl.ds(c * chunk, chunk), :], (((1,), (1,)), ((), ())),
                preferred_element_type=F32) * scale
            sc[c] = s
            return jnp.maximum(top, jnp.max(s, axis=1, keepdims=True))

        top = lax.fori_loop(0, chunks, score, jnp.full((rows, 1), -jnp.inf, F32))
        if cursor[0] < fi_hops - 1:
            hop()
        acc[...] = jnp.zeros_like(acc)

        def gather(c, den):
            e = jnp.exp(sc[c] - top)
            acc[...] += jnp.dot(
                e.astype(BF16), kv[pl.ds(c * chunk, chunk), pl.ds(0, latent_width)],
                preferred_element_type=F32)
            return den + jnp.sum(e, axis=1, keepdims=True)

        den = lax.fori_loop(0, chunks, gather, jnp.zeros((rows, 1), F32))
        lat = (acc[...] / den).astype(BF16)
        one = jnp.dot(lat, vup_ref[:, h * vdim:(h + 1) * vdim], preferred_element_type=F32)
        squares = squares + jnp.sum(one * one, axis=1, keepdims=True)
        gated[:, h * vdim:(h + 1) * vdim] = (one * gain_ref[:, h * vdim:(h + 1) * vdim]).astype(BF16)
        if cursor[0] < fi_hops - 1:
            hop()
    sq_out[...] = jnp.broadcast_to(squares, sq_out.shape)
    local[2].wait()

    tile = total // 4

    @pl.loop(0, 4)
    def _(c):
        cols = pl.ds(pl.multiple_of(c * tile, tile), tile)
        proj[:, cols] = jnp.dot(gated[...], ow[:, cols], preferred_element_type=F32).astype(BF16)

    def block(owner):
        return pl.ds(owner * share, share)

    def t_copy(kind, j, out):
        other = peer(j) if out else me
        mine = me if out else peer(tp - j)
        if kind == 0:
            a, b = sq_out.at[block(other)], sq_in.at[mine]
        elif kind == 1:
            a, b = proj.at[block(other)], red.at[mine]
        else:
            a = b = xs.at[block(mine)]
        return pltpu.make_async_remote_copy(
            a, b, t_send.at[kind, j], t_recv.at[kind, j],
            device_id=(sp, peer(j)), device_id_type=MESH)

    for j in range(1, tp):
        t_copy(0, j, True).start()
        t_copy(1, j, True).start()
    while cursor[0] < fi_hops - 1:
        hop()
    for j in range(1, tp):
        t_copy(0, j, False).wait_recv()
        t_copy(1, j, False).wait_recv()
    summed = proj[block(me), :].astype(F32)
    square = sq_out[block(me), :]
    for j in range(1, tp):
        summed = summed + red[peer(tp - j)].astype(F32)
        square = square + sq_in[peer(tp - j)]
    row_scale = lax.rsqrt(square[:, :1] / (heads * tp * vdim) + EPS)
    middle = stream_ref[...].astype(F32) + row_scale * summed
    mid[...] = middle
    norm = lax.rsqrt(jnp.mean(middle * middle, axis=1, keepdims=True) + EPS)
    xs[block(me), :] = (middle * norm * ngain_ref[...]).astype(BF16)
    for j in range(1, tp):
        t_copy(2, j, True).start()
    hop()
    for j in range(1, tp):
        t_copy(2, j, False).wait_recv()

    wide = 512 if hidden % 512 == 0 else 128

    def first(c):
        cols = pl.ds(pl.multiple_of(c * wide, wide), wide)
        pre = jnp.dot(xs[...], fi[:, cols], preferred_element_type=F32)
        pre = jnp.maximum(pre, 0.0)
        act[:, cols] = (pre * pre).astype(BF16)

    tiles = hidden // wide
    pl.loop(0, tiles // 2)(first)
    advance(1, 1)
    pl.loop(tiles // 2, tiles)(first)

    mixed[sp] = jnp.dot(act[...], fo[sp], preferred_element_type=F32)
    half = hidden // 2

    def part(src, way):
        return jnp.dot(act[:, way * half:(way + 1) * half], fo[src, way * half:(way + 1) * half],
                       preferred_element_type=F32)

    def m_copy(order, src, j, out):
        other = peer(j) if out else me
        mine = me if out else peer(tp - j)
        return pltpu.make_async_remote_copy(
            mix_out.at[src, block(other)], mix_in.at[mine, src],
            m_send.at[order, j], m_recv.at[order, j],
            device_id=(sp, peer(j)), device_id_type=MESH)

    finished = []
    seen = set()

    def finish(offset, src):
        order = len(finished)
        finished.append(src)
        mix_out[src] = mixed[src].astype(BF16)
        for j in range(1, tp):
            m_copy(order, src, j, True).start()

    for step in range(n - 1):
        if step > 0:
            advance(1, step + 1)
        for way in range(2):
            offset = (-1 - step) % n if way == 0 else (1 + step) % n
            src = came(way, step)
            if offset in seen:
                mixed[src] += part(src, way)
                finish(offset, src)
            else:
                seen.add(offset)
                mixed[src] = part(src, way)
        if step == 0:
            finish(0, sp)

    for order, src in enumerate(finished):
        cols = pl.ds(pl.multiple_of(src * dblk, dblk), dblk)
        whole = mix_out[src, block(me), :].astype(F32)
        for j in range(1, tp):
            m_copy(order, src, j, False).wait_recv()
            whole = whole + mix_in[peer(tp - j), src].astype(F32)
        out_ref[:, cols] = (mid[:, cols] + whole).astype(BF16)

    for step in range(n - 1):
        for way in range(2):
            lat_copy(way, step).wait_send()
            par_copy(way, step, core).wait_send()
            for buf in range(2):
                for sub in range(2):
                    w_copy(buf, way, sub, step).wait_send()
    for j in range(1, tp):
        for kind in range(3):
            t_copy(kind, j, True).wait_send()
        for order, src in enumerate(finished):
            m_copy(order, src, j, True).wait_send()


def body(
    n, tp,
    stream, query_nope, query_rope, latent, rope_key, latent_gain,
    key_up, value_up, out_gain, out_weight, norm_gain, ff_in, ff_out,
):
    rows, heads = query_nope.shape[:2]
    width = stream.shape[1]
    latent_width = latent.shape[1]
    rope = rope_key.shape[1]
    pad = -rope % LANES
    dblk, hidden = ff_in.shape
    share = rows // tp
    positions = (lax.axis_index("sp") * rows + jnp.arange(rows, dtype=jnp.int32)).astype(F32)
    lat_full = latent.astype(F32)
    normed = (
        lat_full
        * lax.rsqrt(jnp.mean(lat_full * lat_full, axis=-1, keepdims=True) + EPS)
        * latent_gain
    ).astype(BF16)
    keys_rot = turn(rope_key, positions).astype(BF16)
    query_rot = turn(query_rope, positions).astype(BF16)
    query_lat = jnp.einsum(
        "thn,lhn->htl", query_nope, key_up, preferred_element_type=F32
    ).astype(BF16)
    kv = jnp.concatenate([normed, keys_rot, jnp.zeros((rows, pad), BF16)], axis=1)
    q = jnp.concatenate(
        [query_lat, query_rot.transpose(1, 0, 2), jnp.zeros((heads, rows, pad), BF16)], axis=2
    )
    keys = n * rows
    chunk = 2 * rows if n % 2 == 0 else rows
    vm = pl.BlockSpec(memory_space=pltpu.VMEM)
    hbm = pl.BlockSpec(memory_space=pl.ANY)
    dma = pltpu.SemaphoreType.DMA
    return pl.pallas_call(
        functools.partial(kernel, n, tp, heads, latent_width, width),
        out_shape=jax.ShapeDtypeStruct((share, width), BF16),
        in_specs=[hbm, vm, vm, vm, hbm, vm, vm, hbm, hbm],
        out_specs=vm,
        scratch_shapes=[
            pltpu.VMEM((keys, kv.shape[1]), BF16),
            pltpu.VMEM((width, hidden), BF16),
            pltpu.VMEM((n, hidden, dblk), BF16),
            pltpu.VMEM(out_weight.shape, BF16),
            pltpu.VMEM((keys // chunk, rows, chunk), F32),
            pltpu.VMEM((rows, latent_width), F32),
            pltpu.VMEM((rows, out_weight.shape[0]), BF16),
            pltpu.VMEM((rows, width), BF16),
            pltpu.VMEM((tp, share, width), BF16),
            pltpu.VMEM((rows, LANES), F32),
            pltpu.VMEM((tp, share, LANES), F32),
            pltpu.VMEM((share, width), F32),
            pltpu.VMEM((rows, width), BF16),
            pltpu.VMEM((rows, hidden), BF16),
            pltpu.VMEM((n, rows, dblk), F32),
            pltpu.VMEM((n, rows, dblk), BF16),
            pltpu.VMEM((tp, n, share, dblk), BF16),
            dma((4,)),
            dma((2, n - 1)), dma((2, n - 1)), dma((2, n - 1)), dma((2, n - 1)),
            dma((2, 2, 2, n - 1)), dma((2, 2, 2, n - 1)),
            dma((3, tp)), dma((3, tp)),
            dma((n, tp)), dma((n, tp)),
        ],
        compiler_params=pltpu.CompilerParams(
            collective_id=0, has_side_effects=True, vmem_limit_bytes=63 * 1024 * 1024
        ),
    )(
        kv, q, value_up.reshape(latent_width, -1), out_gain[None, :], out_weight,
        stream, norm_gain[None, :], ff_in, ff_out,
    )


def solution(mesh):
    placed = (
        P(("sp", "tp"), None),
        P("sp", "tp", None),
        P("sp", "tp", None),
        P("sp", None),
        P("sp", None),
        P(),
        P(None, "tp", None),
        P(None, "tp", None),
        P("tp"),
        P("tp", None),
        P(),
        P("sp", "tp"),
        P("tp", "sp"),
    )
    return jax.shard_map(
        functools.partial(body, mesh.shape["sp"], mesh.shape["tp"]),
        mesh=mesh, in_specs=placed, out_specs=P(("sp", "tp"), None), check_vma=False
    )
```

time: 484 us -> 231 us (0.48)
  waiting for transfers between devices: 342 us -> 0 us
  Pallas kernels: 0 us -> 220 us
  matrix products: 59.7 us -> 0.58 us
  blocking collectives: 40.1 us -> 0 us
  other arithmetic: 22.2 us -> 4.46 us
  between operations: 13.6 us -> 0.13 us
    all_gather x4 -> x0, waiting for transfers between devices: 294 us -> none  [the longest x1 127 us: body(): ff_whole = lax.all_gather(ff_out, 'sp', axis=1, tiled=True)]
    pallas_call x0 -> x1, Pallas kernels: none -> 220 us  [body(): pl.pallas_call(functools.partial(kernel, n, tp, heads, latent_width, widt...]
    dot_general x13 -> x1, matrix products: 59.7 us -> 0.58 us  [body(): jnp.einsum('thn,lhn->htl', query_nope, key_up, preferred_element_type=F32)]
    reduce_scatter x2 -> x0, waiting for transfers between devices: 47.4 us -> none  [the longest x1 26.4 us: body(): lax.psum_scatter(jnp.dot(activation, ff_whole, preferred_element_type=jnp...]
    all_gather x1 -> x0, blocking collectives: 34.4 us -> none  [body(): key_piece = lax.all_gather(keys_rot, 'sp', axis=0, tiled=True)]
    reduce_sum x4 -> x0, other arithmetic: 12.6 us -> none  [the longest x3 11.3 us: fold_block(): running_sum = running_sum * fading + jnp.sum(expo, axis=-1)]
    convert_element_type x6 -> x3, other arithmetic: 5.94 us -> 0.07 us  [the longest x2 0.07 us: turn(): vector = values.astype(F32)]
    psum x1 -> x0, blocking collectives: 5.67 us -> none  [body(): square_sums = lax.psum(jnp.sum(head_out * head_out, axis=(1, 2)), 'tp')]
  transfers between devices with their start and end apart: 6 -> 0, of which waited for: 6 -> 0; matrix products, arithmetic and copies ran while one was open for 2% -> 0% of each run, Pallas kernels for 0% -> 0%
where the time goes in v1:
time: 231 us; the launch traced here: 230 us
  Pallas kernels  220 us (95%)
  local copies, waits for them, and re-layouts  5.15 us (2%)
  other arithmetic  4.46 us (2%)
    pallas_call x1, Pallas kernels, body(): pl.pallas_call(functools.partial(kernel, n, tp, heads, latent_width, widt...  220 us
    unnamed x14, local copies, waits for them, and re-layouts  5.07 us

profile of v1, /device:TPU:0, one launch (start us, length us, event | category | flops | bytes accessed | tf_op | source)
XLA Modules:
  0.0 230.5 jit_solution(514191557811481289)
XLA Ops:
  0.0 0.0 copy-start
  0.0 1.0 copy.18
  1.0 0.8 multiply_cosine_fusion
  1.9 1.2 copy.22
  3.0 0.1 convert_element_type.29
  3.1 0.0 copy-start.3
  3.1 0.4 subtract_convert_fusion
  3.5 0.2 maximum_bitcast_fusion
  3.7 0.1 pad.8.clone
  3.8 0.0 copy-done
  3.8 0.3 copy-done.3
  4.1 0.6 convolution_convert_fusion
  4.7 0.0 copy-start.1
  4.7 0.0 copy-start.4
  4.7 1.7 maximum_maximum_fusion.q_ref
  6.4 0.0 copy-start.2
  6.4 0.0 copy-done.1
  6.4 0.2 fusion
  6.6 0.0 copy-done.4
  6.6 0.2 fusion.2
  6.7 0.9 maximum_maximum_fusion.1.kv_ref
  7.7 0.0 copy-done.2
  7.7 0.9 copy.29
  8.5 220.1 %shard_map.127 = bf16[96,2048]{1,0:T(8,128)(2,1)} custom-call(bf16[384,640]{1,0:T(8,128)(2,1)} %maximum_maximum_fusion.1.kv_ref, bf16[4,384,640]{2,1,0:T(8,128)(2,1)} %maximum_maximum_fusion.q_ref, bf16[512,512]{1,0:T(8,128)(2,1)} %bitcast.8, f32[1,512]{1,0:T(1,128)} %bitcast.11, bf16[512,2048]{1,0:T(8,128)(2,1)} %ow_ref.1, bf16[96,2048]{1,0:T(8,128)(2,1)} %stream_ref.1, ...), custom_call_target="tpu_custom_call" | custom-call | tf_op jit(solution)/shard_map/pallas_call | solution.py:394
  228.7 1.8 copy.31
  (5 shorter events, 0.0 us)
Async XLA Ops:
  0.0 3.8 %copy-start = (bf16[512,4,128]{2,1,0:T(4,128)(2,1)S(1)}, bf16[512,4,128]{2,1,0:T(4,128)(2,1)}, u32[]{:S(2)}) copy-start(bf16[512,4,128]{2,1,0:T(4,128)(2,1)} %param.19) | copy-start | bytes 1572868
  3.1 1.0 copy-start.3
  4.7 1.7 copy-start.1
  4.7 1.9 copy-start.4
  6.4 1.3 copy-start.2

commit v2 on v1

--- a/solution.py
+++ b/solution.py
@@ -14,6 +14,7 @@
 BF16 = jnp.bfloat16
 MESH = pl.DeviceIdType.MESH
 LANES = 128
+SUBS = 4
 
 
 def turn(values, positions):
@@ -143,10 +144,10 @@
 
     def w_piece(buf, src, way, sub):
         if buf == 0:
-            part = dblk // 4
-            return fi.at[pl.ds(src * dblk + (2 * way + sub) * part, part)]
-        part = hidden // 4
-        return fo.at[src, pl.ds((2 * way + sub) * part, part)]
+            part = dblk // (2 * SUBS)
+            return fi.at[pl.ds(src * dblk + (SUBS * way + sub) * part, part)]
+        part = hidden // (2 * SUBS)
+        return fo.at[src, pl.ds((SUBS * way + sub) * part, part)]
 
     def w_copy(buf, way, sub, step):
         ref = w_piece(buf, going(way, step), way, sub)
@@ -160,52 +161,51 @@
             ref, ref, w_send.at[buf, way, sub, step], w_recv.at[buf, way, sub, step],
             device_id=(towards[way], me), device_id_type=MESH).wait_recv()
 
-    def advance(buf, step):
-        for sub in range(2):
+    units = [(b, s, u) for b in range(2) for s in range(n - 1) for u in range(SUBS)]
+    ff_in_units = (n - 1) * SUBS
+    cursor = [0]
+    waited = set()
+
+    def need(buf, step, sub):
+        if (buf, step, sub) not in waited:
+            waited.add((buf, step, sub))
             for way in range(2):
-                if step > 0:
-                    w_wait(buf, way, sub, step - 1)
-                if step < n - 1:
-                    w_copy(buf, way, sub, step).start()
+                w_wait(buf, way, sub, step)
+
+    def advance(until):
+        while cursor[0] < min(until, len(units)):
+            buf, step, sub = units[cursor[0]]
+            if step > 0:
+                need(buf, step - 1, sub)
+            for way in range(2):
+                w_copy(buf, way, sub, step).start()
+            cursor[0] += 1
+
+    def one_more(limit):
+        if cursor[0] < limit:
+            advance(cursor[0] + 1)
 
     local[3].wait()
     for way in range(2):
         lat_copy(way, 0).start()
     local[0].wait()
-    local[1].wait()
+    advance(1)
     for step in range(n - 1):
         for way in range(2):
             lat_wait(way, step)
             if step < n - 2:
                 lat_copy(way, step + 1).start()
             par_copy(way, step, core).start()
-        if step == n - 3:
-            advance(0, 0)
+        one_more(ff_in_units)
     for step in range(n - 1):
         for way in range(2):
             par_copy(way, step, 1 - core).wait_recv()
-
-    hops = [(0, s) for s in range(1, n)] + [(1, s) for s in range(0, n)]
-    cursor = [0]
-
-    def hop():
-        buf, step = hops[cursor[0]]
-        if buf == 0 and step == n - 1:
-            cursor[0] += 1
-            advance(1, 0)
-            advance(0, n - 1)
-            cursor[0] += 1
-            return
-        advance(buf, step)
-        cursor[0] += 1
 
     scale = 1.0 / math.sqrt(LANES + (q_ref.shape[2] - latent_width) // 2)
     chunk = sc.shape[2]
     chunks = keys // chunk
     vdim = LANES
     squares = jnp.zeros((rows, 1), F32)
-    fi_hops = n - 1
-    points = 2 * heads
     for h in range(heads):
         def score(c, top):
             s = lax.dot_general(
@@ -215,8 +215,7 @@
             return jnp.maximum(top, jnp.max(s, axis=1, keepdims=True))
 
         top = lax.fori_loop(0, chunks, score, jnp.full((rows, 1), -jnp.inf, F32))
-        if cursor[0] < fi_hops - 1:
-            hop()
+        one_more(ff_in_units)
         acc[...] = jnp.zeros_like(acc)
 
         def gather(c, den):
@@ -231,17 +230,19 @@
         one = jnp.dot(lat, vup_ref[:, h * vdim:(h + 1) * vdim], preferred_element_type=F32)
         squares = squares + jnp.sum(one * one, axis=1, keepdims=True)
         gated[:, h * vdim:(h + 1) * vdim] = (one * gain_ref[:, h * vdim:(h + 1) * vdim]).astype(BF16)
-        if cursor[0] < fi_hops - 1:
-            hop()
+        one_more(ff_in_units)
     sq_out[...] = jnp.broadcast_to(squares, sq_out.shape)
     local[2].wait()
 
     tile = total // 4
 
-    @pl.loop(0, 4)
-    def _(c):
+    def project(c):
         cols = pl.ds(pl.multiple_of(c * tile, tile), tile)
         proj[:, cols] = jnp.dot(gated[...], ow[:, cols], preferred_element_type=F32).astype(BF16)
+
+    pl.loop(0, 2)(project)
+    one_more(ff_in_units)
+    pl.loop(2, 4)(project)
 
     def block(owner):
         return pl.ds(owner * share, share)
@@ -262,8 +263,7 @@
     for j in range(1, tp):
         t_copy(0, j, True).start()
         t_copy(1, j, True).start()
-    while cursor[0] < fi_hops - 1:
-        hop()
+    advance(ff_in_units - SUBS - 2)
     for j in range(1, tp):
         t_copy(0, j, False).wait_recv()
         t_copy(1, j, False).wait_recv()
@@ -279,22 +279,24 @@
     xs[block(me), :] = (middle * norm * ngain_ref[...]).astype(BF16)
     for j in range(1, tp):
         t_copy(2, j, True).start()
-    hop()
+    local[1].wait()
+    advance(ff_in_units + SUBS)
+    for sub in range(SUBS):
+        need(0, n - 2, sub)
     for j in range(1, tp):
         t_copy(2, j, False).wait_recv()
 
     wide = 512 if hidden % 512 == 0 else 128
 
     def first(c):
-        cols = pl.ds(pl.multiple_of(c * wide, wide), wide)
+        cols = pl.ds(c * wide, wide)
         pre = jnp.dot(xs[...], fi[:, cols], preferred_element_type=F32)
         pre = jnp.maximum(pre, 0.0)
         act[:, cols] = (pre * pre).astype(BF16)
 
-    tiles = hidden // wide
-    pl.loop(0, tiles // 2)(first)
-    advance(1, 1)
-    pl.loop(tiles // 2, tiles)(first)
+    for c in range(hidden // wide):
+        first(c)
+        one_more(len(units))
 
     mixed[sp] = jnp.dot(act[...], fo[sp], preferred_element_type=F32)
     half = hidden // 2
@@ -322,8 +324,9 @@
             m_copy(order, src, j, True).start()
 
     for step in range(n - 1):
-        if step > 0:
-            advance(1, step + 1)
+        advance(ff_in_units + (step + 2) * SUBS)
+        for sub in range(SUBS):
+            need(1, step, sub)
         for way in range(2):
             offset = (-1 - step) % n if way == 0 else (1 + step) % n
             src = came(way, step)
@@ -349,7 +352,7 @@
             lat_copy(way, step).wait_send()
             par_copy(way, step, core).wait_send()
             for buf in range(2):
-                for sub in range(2):
+                for sub in range(SUBS):
                     w_copy(buf, way, sub, step).wait_send()
     for j in range(1, tp):
         for kind in range(3):
@@ -416,7 +419,7 @@
             pltpu.VMEM((tp, n, share, dblk), BF16),
             dma((4,)),
             dma((2, n - 1)), dma((2, n - 1)), dma((2, n - 1)), dma((2, n - 1)),
-            dma((2, 2, 2, n - 1)), dma((2, 2, 2, n - 1)),
+            dma((2, 2, SUBS, n - 1)), dma((2, 2, SUBS, n - 1)),
             dma((3, tp)), dma((3, tp)),
             dma((n, tp)), dma((n, tp)),
         ],

time: 231 us -> 204 us (0.88)
  Pallas kernels: 220 us -> 194 us
    pallas_call x1, Pallas kernels: 220 us -> 194 us  [body(): pl.pallas_call(functools.partial(kernel, n, tp, heads, latent_width, widt...]
where the time goes in v2:
time: 204 us
  Pallas kernels  194 us (95%)
  local copies, waits for them, and re-layouts  5.15 us (3%)
  other arithmetic  4.46 us (2%)
    pallas_call x1, Pallas kernels, body(): pl.pallas_call(functools.partial(kernel, n, tp, heads, latent_width, widt...  194 us
    unnamed x14, local copies, waits for them, and re-layouts  5.07 us

profile of v2, /device:TPU:0, one launch (start us, length us, event | category | flops | bytes accessed | tf_op | source)
XLA Modules:
  0.0 203.9 jit_solution(15027641247898533442)
XLA Ops:
  0.0 0.0 copy-start
  0.0 1.0 copy.18
  1.0 0.8 multiply_cosine_fusion
  1.9 1.2 copy.22
  3.0 0.1 convert_element_type.29
  3.1 0.0 copy-start.3
  3.1 0.4 subtract_convert_fusion
  3.5 0.2 maximum_bitcast_fusion
  3.7 0.1 pad.8.clone
  3.8 0.0 copy-done
  3.8 0.3 copy-done.3
  4.1 0.6 convolution_convert_fusion
  4.7 0.0 copy-start.1
  4.7 0.0 copy-start.4
  4.7 1.7 maximum_maximum_fusion.q_ref
  6.4 0.0 copy-start.2
  6.4 0.0 copy-done.1
  6.4 0.2 fusion
  6.6 0.0 copy-done.4
  6.6 0.2 fusion.2
  6.7 0.9 maximum_maximum_fusion.1.kv_ref
  7.7 0.0 copy-done.2
  7.7 0.9 copy.29
  8.5 193.6 %shard_map.127 = bf16[96,2048]{1,0:T(8,128)(2,1)} custom-call(bf16[384,640]{1,0:T(8,128)(2,1)} %maximum_maximum_fusion.1.kv_ref, bf16[4,384,640]{2,1,0:T(8,128)(2,1)} %maximum_maximum_fusion.q_ref, bf16[512,512]{1,0:T(8,128)(2,1)} %bitcast.8, f32[1,512]{1,0:T(1,128)} %bitcast.11, bf16[512,2048]{1,0:T(8,128)(2,1)} %ow_ref.1, bf16[96,2048]{1,0:T(8,128)(2,1)} %stream_ref.1, ...), custom_call_target="tpu_custom_call" | custom-call | tf_op jit(solution)/shard_map/pallas_call | solution.py:397
  202.2 1.8 copy.31
  (5 shorter events, 0.0 us)
Async XLA Ops:
  0.0 3.8 %copy-start = (bf16[512,4,128]{2,1,0:T(4,128)(2,1)S(1)}, bf16[512,4,128]{2,1,0:T(4,128)(2,1)}, u32[]{:S(2)}) copy-start(bf16[512,4,128]{2,1,0:T(4,128)(2,1)} %param.19) | copy-start | bytes 1572868
  3.1 1.0 copy-start.3
  4.7 1.7 copy-start.1
  4.7 1.9 copy-start.4
  6.4 1.3 copy-start.2
